TPU v7x, 128 devices: a whole 4x4x4 slice. The times are simulated.
128 devices in a mesh: sp: 32 (over z, y, core), tp: 4 (over x).
Axes of the slice: x: 4, y: 4, z: 4, core: 2. Of those that a mesh axis runs over, the one named last changes fastest.
Arguments:
- tokens: bfloat16 [4, 2048, 1024], P(None, 'sp', 'tp'), may hold values from -6 to 6
- norm_gain: float32 [4, 1024], replicated, may hold values from 0.1 to 1.9
- val_weight: bfloat16 [4, 1024, 512], P(None, 'sp', 'tp'), may hold values from -0.1875 to 0.1875
- gate_weight: bfloat16 [4, 1024, 512], P(None, 'sp', 'tp'), may hold values from -0.1875 to 0.1875
- conv_taps: float32 [4, 31, 512], P(None, None, 'tp'), may hold values from -1 to 1
- conv_bias: float32 [4, 512], P(None, 'tp'), may hold values from -3 to 3
- ln_gain: float32 [4, 512], P(None, 'tp'), may hold values from 0.1 to 1.9
- ln_shift: float32 [4, 512], P(None, 'tp'), may hold values from -3 to 3
- out_weight: bfloat16 [4, 512, 1024], P(None, 'tp', 'sp'), may hold values from -0.25 to 0.25
Outputs:
- stream: bfloat16 [4, 2048, 1024], P(None, 'sp', 'tp')
All inputs are finite; a program needn't handle non-finite values.
Results may differ from a plain program's by a relative error of at most 0.02.
Values may be sent and summed in bfloat16 or wider, within the bound.
A program may use at most 64 MiB of HBM per device.

v0:
```python
from functools import partial

import jax
import jax.numpy as jnp
from jax import lax
from jax.sharding import PartitionSpec as P

LAYERS = 4


epsilon = 1e-06


def over_all(shard, axis, dim, absorb, state):
    everything = jax.tree.map(lambda a: lax.all_gather(a, axis, axis=dim, tiled=True), shard)
    return absorb(state, everything, jnp.int32(0))


def with_halo(shard, sides, width, wrap):
    for axis, dim in sides:
        size, length = lax.axis_size(axis), shard.shape[dim]
        up = [(i, (i + 1) % size) for i in range(size if wrap else size - 1)]
        down = [(j, i) for i, j in up]
        last = lax.slice_in_dim(shard, length - width, length, axis=dim)
        initial = lax.slice_in_dim(shard, 0, width, axis=dim)
        before = lax.ppermute(last, axis, up)
        after = lax.ppermute(initial, axis, down)
        shard = jnp.concatenate([before, shard, after], axis=dim)
    return shard


def together(arrays, axis):
    ends = [0]
    for a in arrays:
        ends.append(ends[-1] + a.size)
    subtotal = lax.psum(jnp.concatenate([a.ravel() for a in arrays]), axis)
    return tuple(subtotal[b:e].reshape(a.shape) for a, b, e in zip(arrays, ends, ends[1:]))


def on_whole(shard, axis, dim, work):
    return work(lax.all_gather(shard, axis, axis=dim, tiled=True), jnp.int32(0))


def depthwise(padded, tap_weights, length):
    running = padded[:, 0:length] * tap_weights[0]
    for tap_idx in range(1, tap_weights.shape[0]):
        running = running + padded[:, tap_idx : tap_idx + length] * tap_weights[tap_idx]
    return running


def add_rows(left_rows, running, shard_piece, offset):
    columns = lax.dynamic_slice_in_dim(left_rows, offset, shard_piece.shape[0], 1)
    return running + jnp.dot(columns, shard_piece, preferred_element_type=jnp.float32)


def add_both(left_rows, totals, pieces, offset):
    return (
        add_rows(left_rows, totals[0], pieces[0], offset),
        add_rows(left_rows, totals[1], pieces[1], offset),
    )


def project_rows(left_rows, shard_piece, offset):
    return jnp.dot(left_rows, shard_piece, preferred_element_type=jnp.float32)


def shards(
    tokens, norm_gain, val_weight, gate_weight, conv_taps, conv_bias, ln_gain, ln_shift, out_weight
):
    stream = tokens
    num_seqs = tokens.shape[0]
    local_len = tokens.shape[1]
    chan_width = val_weight.shape[2]
    all_channels = chan_width * lax.axis_size("tp")
    half_width = conv_taps.shape[1] // 2
    for layer_idx in range(LAYERS):
        gathered = lax.all_gather(stream, "tp", axis=2, tiled=True)
        widened = gathered.astype(jnp.float32)
        scaled = widened * lax.rsqrt(jnp.mean(widened * widened, axis=-1, keepdims=True) + epsilon)
        normed = (scaled * norm_gain[layer_idx]).astype(jnp.bfloat16)
        tok_rows = normed.reshape(-1, normed.shape[2])
        zeroed = jnp.zeros((tok_rows.shape[0], chan_width), jnp.float32)
        values, gates = over_all(
            (val_weight[layer_idx], gate_weight[layer_idx]),
            "sp",
            0,
            partial(add_both, tok_rows),
            (zeroed, zeroed),
        )
        gated = (
            (values * jax.nn.sigmoid(gates))
            .astype(jnp.bfloat16)
            .reshape(num_seqs, local_len, chan_width)
        )
        padded = with_halo(gated, (("sp", 1),), half_width, False)
        convolved = (
            depthwise(padded.astype(jnp.float32), conv_taps[layer_idx], local_len)
            + conv_bias[layer_idx]
        )
        first_sum, second_sum = together(
            (jnp.sum(convolved, axis=-1), jnp.sum(convolved * convolved, axis=-1)), "tp"
        )
        mean_val = (first_sum / all_channels)[..., None]
        spread = (second_sum / all_channels)[..., None] - mean_val * mean_val
        centered = convolved - mean_val
        normalized = (
            centered * lax.rsqrt(spread + epsilon) * ln_gain[layer_idx] + ln_shift[layer_idx]
        )
        activated = jax.nn.silu(normalized).astype(jnp.bfloat16).reshape(-1, chan_width)
        partial_terms = on_whole(out_weight[layer_idx], "sp", 1, partial(project_rows, activated))
        full_width = partial_terms.shape[1]
        summed = lax.psum_scatter(
            partial_terms.reshape(num_seqs, local_len, full_width).astype(jnp.bfloat16),
            "tp",
            scatter_dimension=2,
            tiled=True,
        ).astype(jnp.float32)
        stream = (stream.astype(jnp.float32) + summed).astype(jnp.bfloat16)
    return stream


def solution(mesh):
    return jax.shard_map(
        shards,
        mesh=mesh,
        in_specs=(
            P(None, "sp", "tp"),
            P(),
            P(None, "sp", "tp"),
            P(None, "sp", "tp"),
            P(None, None, "tp"),
            P(None, "tp"),
            P(None, "tp"),
            P(None, "tp"),
            P(None, "tp", "sp"),
        ),
        out_specs=P(None, "sp", "tp"),
        check_vma=False,
    )
```

profile of v0, /device:TPU:1, one launch (start us, length us, event | category | flops | bytes accessed | tf_op | source)
XLA Modules:
  0.0 451.9 jit_solution(18299880186058381866)
XLA Ops:
  7.4 12.5 %all_gather.48 = bf16[4,64,1024]{2,1,0:T(8,128)(2,1)S(1)} all-gather(bf16[4,64,256]{2,1,0:T(8,128)(2,1)} %param.9), channel_id=1, replica_groups=mesh['sp'=32,'tp'=4] {'tp'}, dimensions={2}, use_global_device_ids=true | all-gather | bytes 655360 | tf_op jit(solution)/shard_map/all_gather | solution.py:77
  20.7 28.5 %all-gather = bf16[1,1024,128]{2,1,0:T(8,128)(2,1)S(1)} all-gather(bf16[1,32,128]{2,1,0:T(8,128)(2,1)S(1)} %get-tuple-element.155), channel_id=2, replica_groups=mesh['sp'=32,'tp'=4] {'sp'}, dimensions={1}, use_global_device_ids=true | all-gather | bytes 270336 | tf_op jit(solution)/shard_map/all_gather | solution.py:15
  49.2 24.1 %all-gather.1 = bf16[1,1024,128]{2,1,0:T(8,128)(2,1)S(1)} all-gather(bf16[1,32,128]{2,1,0:T(8,128)(2,1)S(1)} %get-tuple-element.151), channel_id=3, replica_groups=mesh['sp'=32,'tp'=4] {'sp'}, dimensions={1}, use_global_device_ids=true | all-gather | bytes 270336 | tf_op jit(solution)/shard_map/all_gather | solution.py:15
  74.1 1.9 collective-permute-start
  76.0 2.4 collective-permute-start.1
  79.9 25.7 %all-gather.2 = bf16[1,128,1024]{1,2,0:T(8,128)(2,1)S(1)} all-gather(bf16[1,128,32]{1,2,0:T(8,128)(2,1)S(1)} %get-tuple-element.157), channel_id=4, replica_groups=mesh['sp'=32,'tp'=4] {'sp'}, dimensions={2}, use_global_device_ids=true | all-gather | bytes 270336 | tf_op jit(solution)/shard_map/all_gather | solution.py:41
  106.4 8.7 %psum.28 = f32[512]{0:T(512)S(1)} all-reduce(f32[512]{0:T(512)S(1)} %pad_maximum_fusion), channel_id=1, replica_groups=mesh['sp'=32,'tp'=4] {'tp'}, use_global_device_ids=true, to_apply=%region_3.0 | all-reduce | flops 512 | bytes 4096 | tf_op jit(solution)/shard_map/psum | solution.py:36
  116.5 24.9 %all-gather.3 = bf16[1,1024,128]{2,1,0:T(8,128)(2,1)S(1)} all-gather(bf16[1,32,128]{2,1,0:T(8,128)(2,1)S(1)} %get-tuple-element.154), channel_id=5, replica_groups=mesh['sp'=32,'tp'=4] {'sp'}, dimensions={1}, use_global_device_ids=true | all-gather | bytes 270336 | tf_op jit(solution)/shard_map/all_gather | solution.py:15
  141.4 23.7 %all-gather.4 = bf16[1,1024,128]{2,1,0:T(8,128)(2,1)S(1)} all-gather(bf16[1,32,128]{2,1,0:T(8,128)(2,1)S(1)} %get-tuple-element.150), channel_id=6, replica_groups=mesh['sp'=32,'tp'=4] {'sp'}, dimensions={1}, use_global_device_ids=true | all-gather | bytes 270336 | tf_op jit(solution)/shard_map/all_gather | solution.py:15
  166.1 10.3 %all_gather.52 = bf16[4,64,1024]{2,1,0:T(8,128)(2,1)S(1)} all-gather(bf16[4,64,256]{2,1,0:T(8,128)(2,1)S(1)} %add_convert_fusion.3), channel_id=1, replica_groups=mesh['sp'=32,'tp'=4] {'tp'}, dimensions={2}, use_global_device_ids=true | all-gather | bytes 655360 | tf_op jit(solution)/shard_map/all_gather | solution.py:77
  177.4 5.0 %collective-permute-start.2 = (bf16[4,15,128]{2,1,0:T(8,128)(2,1)S(1)}, bf16[4,15,128]{2,1,0:T(8,128)(2,1)S(1)}, u32[]{:S(2)}, u32[]{:S(2)}) collective-permute-start(bf16[4,15,128]{2,1,0:T(8,128)(2,1)S(1)} %get-tuple-element.21), channel_id=1, source_target_pairs={{0,4},{4,8},{8,12},{12,16},{16,20},{20,24},{24,28},{28,32},{32,36}... | collective-permute-start | bytes 46088 | tf_op jit(solution)/shard_map/ppermute | solution.py:26
  182.4 1.9 collective-permute-start.3
  184.3 27.1 %all-gather.5 = bf16[1,128,1024]{1,2,0:T(8,128)(2,1)S(1)} all-gather(bf16[1,128,32]{1,2,0:T(8,128)(2,1)S(1)} %get-tuple-element.158), channel_id=7, replica_groups=mesh['sp'=32,'tp'=4] {'sp'}, dimensions={2}, use_global_device_ids=true | all-gather | bytes 270336 | tf_op jit(solution)/shard_map/all_gather | solution.py:41
  212.2 6.0 %psum.29 = f32[512]{0:T(512)S(1)} all-reduce(f32[512]{0:T(512)S(1)} %pad_maximum_fusion.1), channel_id=1, replica_groups=mesh['sp'=32,'tp'=4] {'tp'}, use_global_device_ids=true, to_apply=%region_8.9 | all-reduce | flops 512 | bytes 4096 | tf_op jit(solution)/shard_map/psum | solution.py:36
  218.4 1.2 convolution_convert_fusion.2
  219.6 24.1 %all-gather.6 = bf16[1,1024,128]{2,1,0:T(8,128)(2,1)S(1)} all-gather(bf16[1,32,128]{2,1,0:T(8,128)(2,1)S(1)} %get-tuple-element.156), channel_id=8, replica_groups=mesh['sp'=32,'tp'=4] {'sp'}, dimensions={1}, use_global_device_ids=true | all-gather | bytes 270336 | tf_op jit(solution)/shard_map/all_gather | solution.py:15
  243.7 24.1 %all-gather.7 = bf16[1,1024,128]{2,1,0:T(8,128)(2,1)S(1)} all-gather(bf16[1,32,128]{2,1,0:T(8,128)(2,1)S(1)} %get-tuple-element.152), channel_id=9, replica_groups=mesh['sp'=32,'tp'=4] {'sp'}, dimensions={1}, use_global_device_ids=true | all-gather | bytes 270336 | tf_op jit(solution)/shard_map/all_gather | solution.py:15
  268.8 10.3 %all_gather.56 = bf16[4,64,1024]{2,1,0:T(8,128)(2,1)S(1)} all-gather(bf16[4,64,256]{2,1,0:T(8,128)(2,1)S(1)} %add_convert_fusion.2), channel_id=1, replica_groups=mesh['sp'=32,'tp'=4] {'tp'}, dimensions={2}, use_global_device_ids=true | all-gather | bytes 655360 | tf_op jit(solution)/shard_map/all_gather | solution.py:77
  280.1 3.8 collective-permute-start.4
  283.9 2.2 collective-permute-start.5
  286.1 26.7 %all-gather.8 = bf16[1,128,1024]{1,2,0:T(8,128)(2,1)S(1)} all-gather(bf16[1,128,32]{1,2,0:T(8,128)(2,1)S(1)} %get-tuple-element.160), channel_id=10, replica_groups=mesh['sp'=32,'tp'=4] {'sp'}, dimensions={2}, use_global_device_ids=true | all-gather | bytes 270336 | tf_op jit(solution)/shard_map/all_gather | solution.py:41
  313.5 7.9 %psum.30 = f32[512]{0:T(512)S(1)} all-reduce(f32[512]{0:T(512)S(1)} %pad_maximum_fusion.2), channel_id=1, replica_groups=mesh['sp'=32,'tp'=4] {'tp'}, use_global_device_ids=true, to_apply=%region_13.14 | all-reduce | flops 512 | bytes 4096 | tf_op jit(solution)/shard_map/psum | solution.py:36
  321.6 1.2 convolution_convert_fusion.1
  322.9 24.9 %all-gather.9 = bf16[1,1024,128]{2,1,0:T(8,128)(2,1)S(1)} all-gather(bf16[1,32,128]{2,1,0:T(8,128)(2,1)S(1)} %get-tuple-element.153), channel_id=11, replica_groups=mesh['sp'=32,'tp'=4] {'sp'}, dimensions={1}, use_global_device_ids=true | all-gather | bytes 270336 | tf_op jit(solution)/shard_map/all_gather | solution.py:15
  347.8 23.8 %all-gather.10 = bf16[1,1024,128]{2,1,0:T(8,128)(2,1)S(1)} all-gather(bf16[1,32,128]{2,1,0:T(8,128)(2,1)S(1)} %get-tuple-element.149), channel_id=12, replica_groups=mesh['sp'=32,'tp'=4] {'sp'}, dimensions={1}, use_global_device_ids=true | all-gather | bytes 270336 | tf_op jit(solution)/shard_map/all_gather | solution.py:15
  372.5 10.3 %all_gather.60 = bf16[4,64,1024]{2,1,0:T(8,128)(2,1)S(1)} all-gather(bf16[4,64,256]{2,1,0:T(8,128)(2,1)S(1)} %add_convert_fusion.1), channel_id=1, replica_groups=mesh['sp'=32,'tp'=4] {'tp'}, dimensions={2}, use_global_device_ids=true | all-gather | bytes 655360 | tf_op jit(solution)/shard_map/all_gather | solution.py:77
  383.8 5.0 %collective-permute-start.6 = (bf16[4,15,128]{2,1,0:T(8,128)(2,1)S(1)}, bf16[4,15,128]{2,1,0:T(8,128)(2,1)S(1)}, u32[]{:S(2)}, u32[]{:S(2)}) collective-permute-start(bf16[4,15,128]{2,1,0:T(8,128)(2,1)S(1)} %get-tuple-element.17), channel_id=1, source_target_pairs={{0,4},{4,8},{8,12},{12,16},{16,20},{20,24},{24,28},{28,32},{32,36}... | collective-permute-start | bytes 46088 | tf_op jit(solution)/shard_map/ppermute | solution.py:26
  388.8 1.9 collective-permute-start.7
  390.8 26.9 %all-gather.11 = bf16[1,128,1024]{1,2,0:T(8,128)(2,1)S(1)} all-gather(bf16[1,128,32]{1,2,0:T(8,128)(2,1)S(1)} %get-tuple-element.159), channel_id=13, replica_groups=mesh['sp'=32,'tp'=4] {'sp'}, dimensions={2}, use_global_device_ids=true | all-gather | bytes 270336 | tf_op jit(solution)/shard_map/all_gather | solution.py:41
  418.5 6.0 %psum.31 = f32[512]{0:T(512)S(1)} all-reduce(f32[512]{0:T(512)S(1)} %pad_maximum_fusion.3), channel_id=1, replica_groups=mesh['sp'=32,'tp'=4] {'tp'}, use_global_device_ids=true, to_apply=%region_18.19 | all-reduce | flops 512 | bytes 4096 | tf_op jit(solution)/shard_map/psum | solution.py:36
  425.8 18.0 %reduce-scatter.11.cloned.1.call-done = bf16[4,64,256]{2,1,0:T(8,128)(2,1)} async-done(((bf16[4,64,1024]{2,1,0:T(8,128)(2,1)}), bf16[4,64,256]{2,1,0:T(8,128)(2,1)}) %reduce-scatter.11.cloned.1.call-update) | async-done | bytes 131088 | tf_op jit(solution)/shard_map/reduce_scatter | solution.py:112
  443.8 1.6 add_convert_fusion
  (113 shorter events, 16.0 us)
Async XLA Ops:
  6.5 158.6 %reduce-scatter.5.cloned.1.call-start = ((), (), s32[]{:S(2)}) async-start(), calls=%async_computation.4 | async-start | bytes 655360 | tf_op jit(solution)/shard_map/reduce_scatter | solution.py:112
  19.9 0.8 copy-start.2
  20.7 28.5 %copy-start.3 = (bf16[4,32,128]{2,1,0:T(8,128)(2,1)S(1)}, bf16[4,32,128]{2,1,0:T(8,128)(2,1)}, u32[]{:S(2)}) copy-start(bf16[4,32,128]{2,1,0:T(8,128)(2,1)} %param.12) | copy-start | bytes 98308
  74.1 4.4 copy-start.1
  74.1 5.1 %copy-start.4 = (bf16[4,128,32]{1,2,0:T(8,128)(2,1)S(1)}, bf16[4,128,32]{1,2,0:T(8,128)(2,1)}, u32[]{:S(2)}) copy-start(bf16[4,128,32]{1,2,0:T(8,128)(2,1)} %param.17) | copy-start | bytes 98308
  74.1 31.5 %collective-permute-start = (bf16[4,15,128]{2,1,0:T(8,128)(2,1)S(1)}, bf16[4,15,128]{2,1,0:T(8,128)(2,1)S(1)}, u32[]{:S(2)}, u32[]{:S(2)}) collective-permute-start(bf16[4,15,128]{2,1,0:T(8,128)(2,1)S(1)} %get-tuple-element.23), channel_id=1, source_target_pairs={{0,4},{4,8},{8,12},{12,16},{16,20},{20,24},{24,28},{28,32},{32,36}... | collective-permute-start | bytes 46088 | tf_op jit(solution)/shard_map/ppermute | solution.py:26
  76.0 29.6 %collective-permute-start.1 = (bf16[4,15,128]{2,1,0:T(8,128)(2,1)S(1)}, bf16[4,15,128]{2,1,0:T(8,128)(2,1)S(1)}, u32[]{:S(2)}, u32[]{:S(2)}) collective-permute-start(bf16[4,15,128]{2,1,0:T(8,128)(2,1)S(1)} %get-tuple-element.24), channel_id=1, source_target_pairs={{4,0},{8,4},{12,8},{16,12},{20,16},{24,20},{28,24},{32,28},{36,32}... | collective-permute-start | bytes 46088 | tf_op jit(solution)/shard_map/ppermute | solution.py:27
  78.5 0.7 copy-start.5
  79.2 0.7 copy-start.6
  79.2 0.7 copy-start.7
  116.4 151.4 %reduce-scatter.7.cloned.1.call-start = ((), (), s32[]{:S(2)}) async-start(), calls=%async_computation.5 | async-start | bytes 655360 | tf_op jit(solution)/shard_map/reduce_scatter | solution.py:112
  141.4 23.7 %copy-start = (bf16[4,64,256]{2,1,0:T(8,128)(2,1)S(1)}, bf16[4,64,256]{2,1,0:T(8,128)(2,1)}, u32[]{:S(2)}) copy-start(bf16[4,64,256]{2,1,0:T(8,128)(2,1)} %param.9) | copy-start | bytes 393220
  177.4 34.0 %collective-permute-start.2 = (bf16[4,15,128]{2,1,0:T(8,128)(2,1)S(1)}, bf16[4,15,128]{2,1,0:T(8,128)(2,1)S(1)}, u32[]{:S(2)}, u32[]{:S(2)}) collective-permute-start(bf16[4,15,128]{2,1,0:T(8,128)(2,1)S(1)} %get-tuple-element.21), channel_id=1, source_target_pairs={{0,4},{4,8},{8,12},{12,16},{16,20},{20,24},{24,28},{28,32},{32,36}... | collective-permute-start | bytes 46088 | tf_op jit(solution)/shard_map/ppermute | solution.py:26
  182.4 29.0 %collective-permute-start.3 = (bf16[4,15,128]{2,1,0:T(8,128)(2,1)S(1)}, bf16[4,15,128]{2,1,0:T(8,128)(2,1)S(1)}, u32[]{:S(2)}, u32[]{:S(2)}) collective-permute-start(bf16[4,15,128]{2,1,0:T(8,128)(2,1)S(1)} %get-tuple-element.22), channel_id=1, source_target_pairs={{4,0},{8,4},{12,8},{16,12},{20,16},{24,20},{28,24},{32,28},{36,32}... | collective-permute-start | bytes 46088 | tf_op jit(solution)/shard_map/ppermute | solution.py:27
  219.5 152.0 %reduce-scatter.9.cloned.1.call-start = ((), (), s32[]{:S(2)}) async-start(), calls=%async_computation.6 | async-start | bytes 655360 | tf_op jit(solution)/shard_map/reduce_scatter | solution.py:112
  280.1 32.6 %collective-permute-start.4 = (bf16[4,15,128]{2,1,0:T(8,128)(2,1)S(1)}, bf16[4,15,128]{2,1,0:T(8,128)(2,1)S(1)}, u32[]{:S(2)}, u32[]{:S(2)}) collective-permute-start(bf16[4,15,128]{2,1,0:T(8,128)(2,1)S(1)} %get-tuple-element.19), channel_id=1, source_target_pairs={{0,4},{4,8},{8,12},{12,16},{16,20},{20,24},{24,28},{28,32},{32,36}... | collective-permute-start | bytes 46088 | tf_op jit(solution)/shard_map/ppermute | solution.py:26
  283.9 28.9 %collective-permute-start.5 = (bf16[4,15,128]{2,1,0:T(8,128)(2,1)S(1)}, bf16[4,15,128]{2,1,0:T(8,128)(2,1)S(1)}, u32[]{:S(2)}, u32[]{:S(2)}) collective-permute-start(bf16[4,15,128]{2,1,0:T(8,128)(2,1)S(1)} %get-tuple-element.20), channel_id=1, source_target_pairs={{4,0},{8,4},{12,8},{16,12},{20,16},{24,20},{28,24},{32,28},{36,32}... | collective-permute-start | bytes 46088 | tf_op jit(solution)/shard_map/ppermute | solution.py:27
  322.8 121.0 %reduce-scatter.11.cloned.1.call-start = ((), (), s32[]{:S(2)}) async-start(), calls=%async_computation.7 | async-start | bytes 655360 | tf_op jit(solution)/shard_map/reduce_scatter | solution.py:112
  383.8 33.9 %collective-permute-start.6 = (bf16[4,15,128]{2,1,0:T(8,128)(2,1)S(1)}, bf16[4,15,128]{2,1,0:T(8,128)(2,1)S(1)}, u32[]{:S(2)}, u32[]{:S(2)}) collective-permute-start(bf16[4,15,128]{2,1,0:T(8,128)(2,1)S(1)} %get-tuple-element.17), channel_id=1, source_target_pairs={{0,4},{4,8},{8,12},{12,16},{16,20},{20,24},{24,28},{28,32},{32,36}... | collective-permute-start | bytes 46088 | tf_op jit(solution)/shard_map/ppermute | solution.py:26
  388.8 28.9 %collective-permute-start.7 = (bf16[4,15,128]{2,1,0:T(8,128)(2,1)S(1)}, bf16[4,15,128]{2,1,0:T(8,128)(2,1)S(1)}, u32[]{:S(2)}, u32[]{:S(2)}) collective-permute-start(bf16[4,15,128]{2,1,0:T(8,128)(2,1)S(1)} %get-tuple-element.18), channel_id=1, source_target_pairs={{4,0},{8,4},{12,8},{16,12},{20,16},{24,20},{28,24},{32,28},{36,32}... | collective-permute-start | bytes 46088 | tf_op jit(solution)/shard_map/ppermute | solution.py:27
Sparse Core Ops, SparseCore 0:
  116.6 17.4 reduce-scatter.4
  219.7 17.8 reduce-scatter.6
  322.9 17.4 reduce-scatter.8
  425.9 17.8 reduce-scatter.10
where the time goes:
time: 455 us; the launch traced here: 452 us
  blocking collectives  376 us (83%)
  starting transfers between devices  24.3 us (5%)
  waiting for transfers between devices  18.1 us (4%)
  between operations  13.5 us (3%)
  other arithmetic  8.4 us (2%)
  matrix products  7 us (2%)
    all_gather x8, blocking collectives, over_all(): lax.all_gather(a, axis, axis=dim, tiled=True)  198 us
    all_gather x4, blocking collectives, on_whole(): return work(lax.all_gather(shard, axis, axis=dim, tiled=True), jnp.int32(0))  106 us
    all_gather x4, blocking collectives, shards(): gathered = lax.all_gather(stream, 'tp', axis=2, tiled=True)  43.3 us
    psum x4, blocking collectives, together(): subtotal = lax.psum(jnp.concatenate([a.ravel() for a in arrays]), axis)  28.6 us
    reduce_scatter x4, waiting for transfers between devices, shards(): lax.psum_scatter(partial_terms.reshape(num_seqs, local_len, full_width).a...  18 us
    ppermute x4, starting transfers between devices, with_halo(): before = lax.ppermute(last, axis, up)  15.7 us
  transfers between devices with their start and end apart: 12, of which 1 were waited for; matrix products, arithmetic and copies ran while one was open for 0% of the time, Pallas kernels for 0%

commit v1 on v0

v1 whole, which is shorter than its diff:
```python
import functools

import jax
import jax.numpy as jnp
from jax import lax
from jax.experimental import pallas as pl
from jax.experimental.pallas import tpu as pltpu
from jax.sharding import PartitionSpec as P

LAYERS = 4
RING = 4
BLOCK = 64
HALO = 16
FEATS = 256
CHANS = 128
SHARD = 32
TAPS = 31
HALF = 16
EPS = 1e-6
MESH = pl.DeviceIdType.MESH

ORDER = (("x", "y", "z"), ("y", "z", "x"), ("z", "x", "y"))


class Copies:
    def __init__(self, send_sems, recv_sems):
        self.send_sems, self.recv_sems = send_sems, recv_sems
        self.all = []

    def start(self, src, dst, device):
        at = len(self.all)
        copy = pltpu.make_async_remote_copy(
            src_ref=src,
            dst_ref=dst,
            send_sem=self.send_sems.at[at],
            recv_sem=self.recv_sems.at[at],
            device_id=device,
            device_id_type=MESH,
        )
        copy.start()
        self.all.append(copy)
        return copy


def kernel(
    tok_in, gain_in, val_in, gate_in, taps_in, bias_in, lng_in, lns_in, out_in,
    out_ref,
    W, S, taps, chan, gain, gbuf, cbuf, nbuf, abuf, tok, own_taps, obuf,
    local_sems, send_sems, recv_sems,
):
    sp, x = lax.axis_index("sp"), lax.axis_index("tp")
    z, y, c = sp // 8, (sp // 2) % 4, sp % 2
    own = {"x": x, "y": y, "z": z}

    def device(c_=None, **moved):
        at = dict(own)
        for axis, step in moved.items():
            at[axis] = (own[axis] + step) % RING
        return {"sp": at["z"] * 8 + at["y"] * 2 + (c if c_ is None else c_), "tp": at["x"]}

    partner = device(c_=1 - c)
    other = {"sp": (sp + 31 + 2 * c) % 32, "tp": x}
    near = [device(**{axis: step}) for axis in "xyz" for step in (1, 3, 2)]

    barrier = pltpu.get_barrier_semaphore()
    peers = near + [partner, other]
    for peer in peers:
        pl.semaphore_signal(barrier, inc=1, device_id=peer, device_id_type=MESH)

    def wsel(kind, layer, **at):
        return W.at[(kind, layer) + tuple(at.get(a, own[a]) for a in "xzy") + (c,)]

    locals_ = [
        pltpu.make_async_copy(src, dst, local_sems.at[i])
        for i, (src, dst) in enumerate(
            [(ref.at[l], wsel(k, l)) for l in range(LAYERS) for k, ref in enumerate((val_in, gate_in, out_in))]
            + [
                (tok_in, tok),
                (taps_in.at[pl.ds((HALF - 1) * c, HALF)], own_taps),
                (tok_in.at[x], S.at[x, pl.ds(BLOCK, BLOCK)]),
                (taps_in.at[pl.ds((HALF - 1) * c, HALF)], taps.at[c, x]),
                (gain_in, gain),
                (bias_in, chan.at[0, x]),
                (lng_in, chan.at[1, x]),
                (lns_in, chan.at[2, x]),
            ]
        )
    ]
    for copy in locals_:
        copy.start()
    for copy in locals_:
        copy.wait()
    pl.semaphore_wait(barrier, len(peers))

    copies = Copies(send_sems, recv_sems)
    held = {}
    STEPS = (1, 3, 2)

    def p1(layer):
        for kind in range(3):
            axis = ORDER[kind][0]
            for step in STEPS:
                part = wsel(kind, layer)
                held["p1", layer, kind, step] = copies.start(part, part, device(**{axis: step}))

    def p2_first(layer):
        for kind in range(3):
            for step in STEPS:
                held["p1", layer, kind, step].wait_recv()
            a, b, _ = ORDER[kind]
            part = wsel(kind, layer, **{a: pl.ds(0, 4)})
            for step in (1, 3):
                held["p2", layer, kind, step] = copies.start(part, part, device(**{b: step}))

    def p2_second(layer):
        for kind in range(3):
            a, b, _ = ORDER[kind]
            for half, step in ((0, 1), (2, 3)):
                held["p2", layer, kind, step].wait_recv()
                part = wsel(kind, layer, **{a: pl.ds(half, 2), b: (own[b] + 4 - step) % 4})
                held["p2f", layer, kind, step] = copies.start(part, part, device(**{b: step}))

    def across(layer, kind, at):
        a, b, d = ORDER[kind]
        part = wsel(kind, layer, **{a: pl.ds(0, 4), b: pl.ds(0, 4), d: at})
        held["d2d", layer].append(copies.start(part, part, partner))

    def p3_first(layer):
        held["d2d", layer] = []
        for kind in range(3):
            a, b, d = ORDER[kind]
            for step in (1, 3):
                held["p2f", layer, kind, step].wait_recv()
            part = wsel(kind, layer, **{a: pl.ds(0, 4), b: pl.ds(0, 4)})
            for step in (1, 3):
                held["p3", layer, kind, step] = copies.start(part, part, device(**{d: step}))
            across(layer, kind, own[d])

    def p3_second(layer):
        for kind in range(3):
            a, b, d = ORDER[kind]
            for half, step in ((0, 1), (2, 3)):
                held["p3", layer, kind, step].wait_recv()
                at = (own[d] + 4 - step) % 4
                part = wsel(kind, layer, **{a: pl.ds(half, 2), b: pl.ds(0, 4), d: at})
                held["p3f", layer, kind, step] = copies.start(part, part, device(**{d: step}))
                across(layer, kind, at)

    def p3_last(layer):
        for kind in range(3):
            d = ORDER[kind][2]
            for step in (1, 3):
                held["p3f", layer, kind, step].wait_recv()
            across(layer, kind, (own[d] + 2) % 4)

    def tokens_send():
        for step in STEPS:
            to = (x + step) % 4
            held["tok", step] = copies.start(tok.at[to], S.at[x, pl.ds(BLOCK, BLOCK)], device(x=step))

    def halo_send():
        for step in STEPS:
            held["tok", step].wait_recv()
        block = S.at[:, pl.ds(BLOCK, BLOCK)]
        held["halo"] = [
            copies.start(block, S.at[:, pl.ds(pl.multiple_of(row, BLOCK), BLOCK)], to)
            for row, to in ((2 * BLOCK * c, partner), (2 * BLOCK * (1 - c), other))
        ]

    def params_send():
        held["par"], held["tap"] = [], []
        for step in STEPS:
            held["tap"].append(copies.start(own_taps, taps.at[c, x], device(x=step)))
            for ref, i in ((bias_in, 0), (lng_in, 1), (lns_in, 2)):
                held["par"].append(copies.start(ref, chan.at[i, x], device(x=step)))

    def params_across():
        for copy in held["tap"]:
            copy.wait_recv()
        held["par"].append(copies.start(taps.at[c], taps.at[c], partner))

    row_at = lax.broadcasted_iota(jnp.int32, (3 * BLOCK, CHANS), 0) + (sp * BLOCK - BLOCK)
    inside = jnp.logical_and(row_at >= 0, row_at < 32 * BLOCK)

    def compute(layer):
        r0, rows = HALO * layer, 3 * BLOCK - 2 * HALO * layer
        o0, outs = r0 + HALO, rows - 2 * HALO
        for copy in held["d2d", layer]:
            copy.wait_recv()

        wide = [S[f, r0 : r0 + rows].astype(jnp.float32) for f in range(4)]
        square = wide[0] * wide[0] + wide[1] * wide[1] + wide[2] * wide[2] + wide[3] * wide[3]
        scale = lax.rsqrt(jnp.sum(square, axis=-1, keepdims=True) * (1.0 / (4 * FEATS)) + EPS)
        for f in range(4):
            g = gain[layer : layer + 1, f * FEATS : (f + 1) * FEATS]
            nbuf[r0 : r0 + rows, f * FEATS : (f + 1) * FEATS] = (wide[f] * scale * g).astype(jnp.bfloat16)

        def channel_block(b, carry):
            lhs = nbuf[r0 : r0 + rows]
            rhs = jnp.concatenate(
                [W[k, layer, b].reshape(4 * FEATS, CHANS) for k in (0, 1)], axis=1
            )
            both = jnp.dot(lhs, rhs, preferred_element_type=jnp.float32)
            gated = (both[:, :CHANS] * jax.nn.sigmoid(both[:, CHANS:])).astype(jnp.bfloat16)
            gated = jnp.where(inside[r0 : r0 + rows], gated.astype(jnp.float32), 0.0)
            gbuf[b, r0 : r0 + rows] = gated
            return carry

        lax.fori_loop(0, 4, channel_block, 0)

        def conv_block(b, carry):
            total = jnp.broadcast_to(chan[0, b, layer : layer + 1], (outs, CHANS))
            for k in range(TAPS):
                if k < HALF:
                    t = taps[0, b, k, layer : layer + 1]
                else:
                    t = taps[1, b, k - HALF + 1, layer : layer + 1]
                total = total + gbuf[b, o0 - 15 + k : o0 - 15 + k + outs] * t
            cbuf[b, :outs] = total
            return carry

        lax.fori_loop(0, 4, conv_block, 0)

        conv = [cbuf[b, :outs] for b in range(4)]
        mean = jnp.sum(conv[0] + conv[1] + conv[2] + conv[3], axis=-1, keepdims=True) * (1.0 / 512)
        cent = [v - mean for v in conv]
        square = cent[0] * cent[0] + cent[1] * cent[1] + cent[2] * cent[2] + cent[3] * cent[3]
        scale = lax.rsqrt(jnp.sum(square, axis=-1, keepdims=True) * (1.0 / 512) + EPS)
        for b in range(4):
            n = cent[b] * scale * chan[1, b, layer : layer + 1] + chan[2, b, layer : layer + 1]
            abuf[:outs, b * CHANS : (b + 1) * CHANS] = (n * jax.nn.sigmoid(n)).astype(jnp.bfloat16)

        def out_block(f):
            rhs = jnp.concatenate(
                [W[2, layer, b, f].reshape(FEATS, CHANS) for b in range(4)], axis=1
            )
            branch = lax.dot_general(
                abuf[:outs], rhs, (((1,), (1,)), ((), ())), preferred_element_type=jnp.float32
            )
            return (S[f, o0 : o0 + outs].astype(jnp.float32) + branch).astype(jnp.bfloat16)

        if layer < LAYERS - 1:

            def update(f, carry):
                S[f, o0 : o0 + outs] = out_block(f)
                return carry

            lax.fori_loop(0, 4, update, 0)
        else:
            held["out"] = []
            waiting = []
            for step in (2, 1, 3, 0):
                to = (x + step) % 4
                value = out_block(to)
                if step:
                    obuf[step - 1] = value
                else:
                    out_ref[x] = value
                for s in waiting:
                    held["out"].append(copies.start(obuf.at[s - 1], out_ref.at[x], device(x=s)))
                waiting = [step] if step else []

    p1(0)
    tokens_send()
    p1(1)
    p2_first(0)
    p1(2)
    p1(3)
    p2_second(0)
    p2_first(1)
    params_send()
    halo_send()
    p3_first(0)
    p2_second(1)
    p2_first(2)
    p2_first(3)
    p3_first(1)
    p3_second(0)
    p2_second(2)
    p2_second(3)
    params_across()
    p3_first(2)
    p3_last(0)
    for copy in held["halo"] + held["par"]:
        copy.wait_recv()
    for copy in held["halo"]:
        copy.wait_send()
    compute(0)
    p3_second(1)
    p3_first(3)
    p3_last(1)
    compute(1)
    p3_second(2)
    p3_last(2)
    p3_second(3)
    compute(2)
    p3_last(3)
    compute(3)
    for copy in held["out"]:
        copy.wait_recv()
    for copy in copies.all:
        if all(copy is not done for done in held["halo"]):
            copy.wait_send()


def shards(tokens, norm_gain, val_weight, gate_weight, conv_taps, conv_bias, ln_gain, ln_shift, out_weight):
    copies = 320
    return pl.pallas_call(
        kernel,
        out_shape=jax.ShapeDtypeStruct(tokens.shape, jnp.bfloat16),
        in_specs=[pl.BlockSpec(memory_space=pl.ANY)] * 5
        + [pl.BlockSpec(memory_space=pltpu.VMEM)] * 3
        + [pl.BlockSpec(memory_space=pl.ANY)],
        out_specs=pl.BlockSpec(memory_space=pltpu.VMEM),
        scratch_shapes=[
            pltpu.VMEM((3, LAYERS, 4, 4, 4, 2, SHARD, CHANS), jnp.bfloat16),
            pltpu.VMEM((4, 3 * BLOCK, FEATS), jnp.bfloat16),
            pltpu.VMEM((2, 4, HALF, LAYERS, CHANS), jnp.float32),
            pltpu.VMEM((3, 4, LAYERS, CHANS), jnp.float32),
            pltpu.VMEM((LAYERS, 4 * FEATS), jnp.float32),
            pltpu.VMEM((4, 3 * BLOCK, CHANS), jnp.float32),
            pltpu.VMEM((4, 3 * BLOCK, CHANS), jnp.float32),
            pltpu.VMEM((3 * BLOCK, 4 * FEATS), jnp.bfloat16),
            pltpu.VMEM((3 * BLOCK, 4 * CHANS), jnp.bfloat16),
            pltpu.VMEM((4, BLOCK, FEATS), jnp.bfloat16),
            pltpu.VMEM((HALF, LAYERS, CHANS), jnp.float32),
            pltpu.VMEM((3, BLOCK, FEATS), jnp.bfloat16),
            pltpu.SemaphoreType.DMA((20,)),
            pltpu.SemaphoreType.DMA((copies,)),
            pltpu.SemaphoreType.DMA((copies,)),
        ],
        compiler_params=pltpu.CompilerParams(
            collective_id=0, has_side_effects=True, vmem_limit_bytes=40 * 1024 * 1024
        ),
    )(
        tokens,
        norm_gain,
        val_weight,
        gate_weight,
        jnp.transpose(conv_taps, (1, 0, 2)),
        conv_bias,
        ln_gain,
        ln_shift,
        jnp.transpose(out_weight, (0, 2, 1)),
    )


def solution(mesh):
    return jax.shard_map(
        shards,
        mesh=mesh,
        in_specs=(
            P(None, "sp", "tp"),
            P(),
            P(None, "sp", "tp"),
            P(None, "sp", "tp"),
            P(None, None, "tp"),
            P(None, "tp"),
            P(None, "tp"),
            P(None, "tp"),
            P(None, "tp", "sp"),
        ),
        out_specs=P(None, "sp", "tp"),
        check_vma=False,
    )
```

time: 455 us -> 74.2 us (0.16)
  blocking collectives: 376 us -> 0 us
  Pallas kernels: 0 us -> 66.2 us
  starting transfers between devices: 24.3 us -> 0 us
  waiting for transfers between devices: 18.1 us -> 0 us
  between operations: 13.5 us -> 0.02 us
  other arithmetic: 8.4 us -> 0 us
  matrix products: 7 us -> 0 us
    all_gather x16 -> x0, blocking collectives: 348 us -> none  [the longest x8 198 us: over_all(): lax.all_gather(a, axis, axis=dim, tiled=True)]
    pallas_call x0 -> x1, Pallas kernels: none -> 66.2 us  [shards(): pl.pallas_call(kernel, out_shape=jax.ShapeDtypeStruct(tokens.shape, jnp.b...]
    psum x4 -> x0, blocking collectives: 28.6 us -> none  [together(): subtotal = lax.psum(jnp.concatenate([a.ravel() for a in arrays]), axis)]
    ppermute x8 -> x0, starting transfers between devices: 24.1 us -> none  [the longest x4 15.7 us: with_halo(): before = lax.ppermute(last, axis, up)]
    reduce_scatter x4 -> x0, waiting for transfers between devices: 18 us -> none  [shards(): lax.psum_scatter(partial_terms.reshape(num_seqs, local_len, full_width).a...]
    dot_general x12 -> x0, matrix products: 7 us -> none  [the longest x4 4.66 us: project_rows(): return jnp.dot(left_rows, shard_piece, preferred_element_type=jnp.float32)]
    unnamed x16 -> x19, local copies, waits for them, and re-layouts: 1.92 us -> 7.43 us
    convert_element_type x12 -> x0, other arithmetic: 5.28 us -> none  [the longest x4 4.41 us: shards(): stream = (stream.astype(jnp.float32) + summed).astype(jnp.bfloat16)]
  transfers between devices with their start and end apart: 12 -> 0, of which waited for: 1 -> 0; matrix products, arithmetic and copies ran while one was open for 0% -> 0% of each run, Pallas kernels for 0% -> 0%
where the time goes in v1:
time: 74.2 us; the launch traced here: 73.7 us
  Pallas kernels  66.2 us (89%)
  local copies, waits for them, and re-layouts  7.43 us (10%)
    pallas_call x1, Pallas kernels, shards(): pl.pallas_call(kernel, out_shape=jax.ShapeDtypeStruct(tokens.shape, jnp.b...  66.2 us
    unnamed x19, local copies, waits for them, and re-layouts  7.43 us

profile of v1, /device:TPU:1, one launch (start us, length us, event | category | flops | bytes accessed | tf_op | source)
XLA Modules:
  0.0 73.7 jit_solution(16459106713577606280)
XLA Ops:
  0.0 0.0 copy-start.6
  0.0 0.7 copy-done.6
  0.7 0.0 copy-start
  0.7 0.9 %copy-done = bf16[4,64,256]{2,1,0:T(8,128)(2,1)S(1)} copy-done((bf16[4,64,256]{2,1,0:T(8,128)(2,1)S(1)}, bf16[4,64,256]{2,1,0:T(8,128)(2,1)}, u32[]{:S(2)}) %copy-start) | copy-done | bytes 131096
  1.6 0.0 copy-start.1
  1.6 0.8 %copy-done.1 = f32[4,31,128]{2,0,1:T(4,128)S(1)} copy-done((f32[4,31,128]{2,0,1:T(4,128)S(1)}, f32[4,31,128]{2,0,1:T(4,128)}, u32[]{:S(2)}) %copy-start.1) | copy-done | bytes 63512
  2.4 0.0 copy-start.2
  2.4 0.8 %copy-done.2 = bf16[4,32,128]{2,1,0:T(8,128)(2,1)S(1)} copy-done((bf16[4,32,128]{2,1,0:T(8,128)(2,1)S(1)}, bf16[4,32,128]{2,1,0:T(8,128)(2,1)}, u32[]{:S(2)}) %copy-start.2) | copy-done | bytes 32792
  3.2 0.0 copy-start.3
  3.2 0.8 %copy-done.3 = bf16[4,32,128]{2,1,0:T(8,128)(2,1)S(1)} copy-done((bf16[4,32,128]{2,1,0:T(8,128)(2,1)S(1)}, bf16[4,32,128]{2,1,0:T(8,128)(2,1)}, u32[]{:S(2)}) %copy-start.3) | copy-done | bytes 32792
  3.9 0.0 copy-start.4
  3.9 0.8 %copy-done.4 = bf16[4,128,32]{1,2,0:T(8,128)(2,1)S(1)} copy-done((bf16[4,128,32]{1,2,0:T(8,128)(2,1)S(1)}, bf16[4,128,32]{1,2,0:T(8,128)(2,1)}, u32[]{:S(2)}) %copy-start.4) | copy-done | bytes 32792
  4.7 0.0 copy-start.5
  4.7 0.7 copy-done.5
  5.4 0.0 copy-start.7
  5.4 0.7 copy-done.7
  6.1 0.0 copy-start.8
  6.1 0.7 copy-done.8
  6.8 66.2 %shard_map.91 = bf16[4,64,256]{2,1,0:T(8,128)(2,1)S(1)} custom-call(bf16[4,64,256]{2,1,0:T(8,128)(2,1)S(1)} %copy-done, f32[4,1024]{1,0:T(4,128)S(1)} %copy-done.5, bf16[4,32,128]{2,1,0:T(8,128)(2,1)S(1)} %copy-done.2, bf16[4,32,128]{2,1,0:T(8,128)(2,1)S(1)} %copy-done.3, f32[31,4,128]{2,1,0:T(4,128)S(1)} %bitcast.2, f32[4,128]{1,0:T(4,128)S(1)} %copy-done.6, ...), custom_call_target="tpu_custom_call" | custom-call | tf_op jit(solution)/shard_map/pallas_call | solution.py:308
  73.0 0.7 copy.11
Async XLA Ops:
  0.0 0.7 copy-start.6
  0.7 0.9 %copy-start = (bf16[4,64,256]{2,1,0:T(8,128)(2,1)S(1)}, bf16[4,64,256]{2,1,0:T(8,128)(2,1)}, u32[]{:S(2)}) copy-start(bf16[4,64,256]{2,1,0:T(8,128)(2,1)} %tok_in.1) | copy-start | bytes 393220
  1.6 0.8 %copy-start.1 = (f32[4,31,128]{2,0,1:T(4,128)S(1)}, f32[4,31,128]{2,0,1:T(4,128)}, u32[]{:S(2)}) copy-start(f32[4,31,128]{2,0,1:T(4,128)} %param.13) | copy-start | bytes 190468
  2.4 0.8 %copy-start.2 = (bf16[4,32,128]{2,1,0:T(8,128)(2,1)S(1)}, bf16[4,32,128]{2,1,0:T(8,128)(2,1)}, u32[]{:S(2)}) copy-start(bf16[4,32,128]{2,1,0:T(8,128)(2,1)} %val_in.1) | copy-start | bytes 98308
  3.2 0.8 %copy-start.3 = (bf16[4,32,128]{2,1,0:T(8,128)(2,1)S(1)}, bf16[4,32,128]{2,1,0:T(8,128)(2,1)}, u32[]{:S(2)}) copy-start(bf16[4,32,128]{2,1,0:T(8,128)(2,1)} %gate_in.1) | copy-start | bytes 98308
  3.9 0.8 %copy-start.4 = (bf16[4,128,32]{1,2,0:T(8,128)(2,1)S(1)}, bf16[4,128,32]{1,2,0:T(8,128)(2,1)}, u32[]{:S(2)}) copy-start(bf16[4,128,32]{1,2,0:T(8,128)(2,1)} %param.17) | copy-start | bytes 98308
  4.7 0.7 copy-start.5
  5.4 0.7 copy-start.7
  6.1 0.7 copy-start.8
